TPU v7x, 32 devices: a whole 2x2x4 slice. The times are simulated.
32 devices in a mesh: sp: 8 (over z, x), tp: 4 (over y, core).
Axes of the slice: x: 2, y: 2, z: 4, core: 2. Of those that a mesh axis runs over, the one named last changes fastest.
Arguments:
- tokens: bfloat16 [8192, 4096], P(('sp', 'tp')), may hold values from -6 to 6
- norm_gain: float32 [4096], replicated, may hold values from 0.1 to 1.9
- q_down: bfloat16 [4096, 768], replicated, may hold values from -0.09375 to 0.09375
- kv_down: bfloat16 [4096, 512], replicated, may hold values from -0.09375 to 0.09375
- rope_down: bfloat16 [4096, 32], replicated, may hold values from -8 to 8
- q_gain: float32 [768], replicated, may hold values from 0.1 to 1.9
- kv_gain: float32 [512], replicated, may hold values from 0.1 to 1.9
- q_up: bfloat16 [768, 1536], P(None, 'tp'), may hold values from -0.21875 to 0.21875
- kv_up: bfloat16 [512, 2048], P(None, 'tp'), may hold values from -0.25 to 0.25
- out_weight: bfloat16 [1024, 4096], replicated, may hold values from -0.1875 to 0.1875
- out_gain: float32 [4096], replicated, may hold values from 0.1 to 1.9
Outputs:
- mixed: bfloat16 [8192, 4096], P(('sp', 'tp'))
All inputs are finite; a program needn't handle non-finite values.
Results may differ from a plain program's by a relative error of at most 0.02.
The roundings to bfloat16 on the way count: a program that leaves them out, or rounds other values in their place, can miss the bound.
Values may be sent and summed in bfloat16 or wider, within the bound.
A program may use at most 128 MiB of HBM per device.

v0:
```python
import jax
import jax.numpy as jnp
from jax import lax
from jax.sharding import PartitionSpec as P

NOPE = 64
ROPE = 32
VDIM = 64
EPS = 1e-06
THETA = 500000.0


def scaled_norm(values_in, gain):
    values_in = values_in.astype(jnp.float32)
    return (
        values_in * lax.rsqrt(jnp.mean(values_in * values_in, axis=-1, keepdims=True) + EPS) * gain
    )


def rotate(values_in, position):
    width = values_in.shape[-1]
    half_dim = width // 2
    inverse = 1.0 / THETA ** (jnp.arange(0, width, 2, dtype=jnp.float32) / width)
    angles = position[:, None] * inverse[None, :]
    angles = angles.reshape((angles.shape[0],) + (1,) * (values_in.ndim - 2) + (half_dim,))
    cosine = jnp.cos(angles)
    sine = jnp.sin(angles)
    left = values_in[..., :half_dim]
    right = values_in[..., half_dim:]
    return jnp.concatenate([left * cosine - right * sine, right * cosine + left * sine], axis=-1)


def local(
    tokens,
    norm_gain,
    q_down,
    kv_down,
    rope_down,
    q_gain,
    kv_gain,
    q_up,
    kv_up,
    out_weight,
    out_gain,
):
    row_count = tokens.shape[0]
    tp_count = lax.axis_size("tp")
    tp_place = lax.axis_index("tp")
    sp_place = lax.axis_index("sp")
    group_rows = row_count * tp_count
    row_first = (sp_place * tp_count + tp_place) * row_count
    own_position = (row_first + jnp.arange(row_count)).astype(jnp.float32)
    normed = scaled_norm(tokens, norm_gain).astype(jnp.bfloat16)
    q_lat = scaled_norm(jnp.dot(normed, q_down, preferred_element_type=jnp.float32), q_gain).astype(
        jnp.bfloat16
    )
    kv_lat = scaled_norm(
        jnp.dot(normed, kv_down, preferred_element_type=jnp.float32), kv_gain
    ).astype(jnp.bfloat16)
    key_rot = rotate(
        jnp.dot(normed, rope_down, preferred_element_type=jnp.float32), own_position
    ).astype(jnp.bfloat16)
    q_group, kv_group, rot_group = (
        lax.all_gather(q_lat, "tp", axis=0, tiled=True),
        lax.all_gather(kv_lat, "tp", axis=0, tiled=True),
        lax.all_gather(key_rot, "tp", axis=0, tiled=True),
    )
    query_first = sp_place * group_rows
    query_index = query_first + jnp.arange(group_rows)
    head_count = q_up.shape[1] // (NOPE + ROPE)
    query = jnp.dot(q_group, q_up, preferred_element_type=jnp.float32).reshape(
        group_rows, head_count, NOPE + ROPE
    )
    query = jnp.concatenate(
        [query[..., :NOPE], rotate(query[..., NOPE:], query_index.astype(jnp.float32))], axis=-1
    )
    query = query.astype(jnp.bfloat16)
    query_nope = query[..., :NOPE]
    query_rot = query[..., NOPE:]
    factor = (NOPE + ROPE) ** (-0.5)

    def attend_block(state, key_rows, rot_rows, block_first):

        def compute(state_in):
            top_score, total, summed = state_in
            keys_values = jnp.dot(key_rows, kv_up, preferred_element_type=jnp.float32).astype(
                jnp.bfloat16
            )
            keys_values = keys_values.reshape(key_rows.shape[0], head_count, NOPE + VDIM)
            scores = jnp.einsum(
                "qhd,khd->hqk",
                query_nope,
                keys_values[..., :NOPE],
                preferred_element_type=jnp.float32,
            )
            scores = scores + jnp.einsum(
                "qhd,kd->hqk", query_rot, rot_rows, preferred_element_type=jnp.float32
            )
            scores = scores * factor
            key_index = block_first + jnp.arange(key_rows.shape[0])
            visible = (key_index[None, :] <= query_index[:, None])[None]
            scores = jnp.where(visible, scores, -1e30)
            new_top = jnp.maximum(top_score, jnp.max(scores, axis=-1))
            correction = jnp.exp(top_score - new_top)
            weights = jnp.where(visible, jnp.exp(scores - new_top[..., None]), 0.0)
            total_new = total * correction + jnp.sum(weights, axis=-1)
            product = jnp.einsum(
                "hqk,khd->hqd",
                weights.astype(jnp.bfloat16),
                keys_values[..., NOPE:],
                preferred_element_type=jnp.float32,
            )
            return (new_top, total_new, summed * correction[..., None] + product)

        return lax.cond(
            block_first <= query_first + group_rows - 1, compute, lambda state_in: state_in, state
        )

    start_state = (
        jnp.full((head_count, group_rows), -1e30, jnp.float32),
        jnp.zeros((head_count, group_rows), jnp.float32),
        jnp.zeros((head_count, group_rows, VDIM), jnp.float32),
    )
    key_piece = lax.all_gather(kv_group, "sp", axis=0, tiled=True)
    rot_piece = lax.all_gather(rot_group, "sp", axis=0, tiled=True)
    piece_rows = rot_piece.shape[0]
    block_count = piece_rows // group_rows
    key_blocks = key_piece.reshape((block_count, group_rows) + key_piece.shape[1:])
    rot_blocks = rot_piece.reshape(block_count, group_rows, rot_piece.shape[1])

    def step(state_in, index):
        block_first = index * group_rows
        return (attend_block(state_in, key_blocks[index], rot_blocks[index], block_first), None)

    state_out, unused = lax.scan(step, start_state, jnp.arange(block_count))
    top_score, total, summed = state_out
    attended = (summed / total[..., None]).transpose(1, 0, 2).reshape(group_rows, head_count * VDIM)
    attended = attended.astype(jnp.bfloat16)
    own_heads = lax.all_to_all(attended, "tp", split_axis=0, concat_axis=1, tiled=True)
    projected = jnp.dot(own_heads, out_weight, preferred_element_type=jnp.float32)
    return scaled_norm(projected, out_gain).astype(jnp.bfloat16)


def solution(mesh):
    return jax.shard_map(
        local,
        mesh=mesh,
        in_specs=(
            P(("sp", "tp"), None),
            P(),
            P(),
            P(),
            P(),
            P(),
            P(),
            P(None, "tp"),
            P(None, "tp"),
            P(),
            P(),
        ),
        out_specs=P(("sp", "tp"), None),
        check_vma=False,
    )
```

profile of v0, /device:TPU:26, one launch (start us, length us, event | category | flops | bytes accessed | tf_op | source)
XLA Modules:
  0.0 503.1 jit_solution(1699244683318475322)
XLA Ops:
  6.5 2.1 fusion.22
  8.7 4.4 multiply_reduce_fusion.2
  14.1 4.7 multiply_reduce_fusion.1
  19.8 12.0 %all-gather.4.cloned.1.call-done = bf16[1024,512]{1,0:T(8,128)(2,1)} async-done(((bf16[256,512]{1,0:T(8,128)(2,1)}), bf16[1024,512]{1,0:T(8,128)(2,1)}) %all-gather.4.cloned.1.call-update) | async-done | bytes 1048592 | tf_op jit(solution)/shard_map/all_gather | solution.py:65
  32.8 5.2 %all_gather.18 = bf16[1024,32]{0,1:T(8,128)(2,1)S(1)} all-gather(bf16[256,32]{0,1:T(8,128)(2,1)S(1)} %pad_maximum_fusion.1), channel_id=1, replica_groups=mesh['sp'=8,'tp'=4] {'tp'}, dimensions={0}, use_global_device_ids=true | all-gather | bytes 81920 | tf_op jit(solution)/shard_map/all_gather | solution.py:66
  38.0 32.3 %all_gather.19 = bf16[8192,32]{0,1:T(8,128)(2,1)S(1)} all-gather(bf16[1024,32]{0,1:T(8,128)(2,1)S(1)} %all_gather.18), channel_id=1, replica_groups=mesh['sp'=8,'tp'=4] {'sp'}, dimensions={0}, use_global_device_ids=true | all-gather | bytes 589824 | tf_op jit(solution)/shard_map/all_gather | solution.py:125
  71.5 2.2 fusion.41
  73.9 102.8 %all-gather.6.cloned.1.call-done = bf16[8192,512]{1,0:T(8,128)(2,1)} async-done(((bf16[1024,512]{1,0:T(8,128)(2,1)}), bf16[8192,512]{1,0:T(8,128)(2,1)}) %all-gather.6.cloned.1.call-update) | async-done | bytes 8388624 | tf_op jit(solution)/shard_map/all_gather | solution.py:124
  177.9 297.7 %while.17 = (s32[]{:T(128)}, f32[4,1024]{1,0:T(4,128)S(1)}, f32[4,1024]{1,0:T(4,128)S(1)}, f32[4,1024,64]{1,2,0:T(8,128)}, s32[8]{0:T(128)S(1)}, /*index=5*/s32[...) while((s32[]{:T(128)}, f32[4,1024]{1,0:T(4,128)S(1)}, ...), condition=%wide.region_8.9_spmd.clone, body=%wide.region_3.8_spmd.clone.sunk | while | flops 1923098624 | bytes 107569616 | solution.py:135
  179.0 36.1 %conditional.3 = ((f32[4,1024]{1,0:T(4,128)S(1)}, f32[4,1024]{1,0:T(4,128)S(1)}, f32[4,1024,64]{1,2,0:T(8,128)})) conditional(s32[]{:T(128)} %convert_element_type.106, (f32[4,1024]{1,0:T(4,128)S(1)}, f32[4,1024]{1,0:T(4,128)S(1)}, f32[4,1024,64]{1,2,0:T(8,128)}) %tuple.62, (s32[]{:T(128)}, s32[]{:T(128)}, s32[]{:T(128)}, ...), branch_computations={%region_4.4_spmd, %region_5.7_spmd} | conditional | flops 1923098624 | bytes 107565224 | solution.py:115
  180.8 1.7 broadcast_compare_fusion
  182.5 2.1 convolution_convert_fusion
  185.6 2.4 fusion.15
  187.9 9.2 %fusion.40 = (f32[4,1024]{1,0:T(4,128)S(1)}, f32[4,1024,1024]{1,2,0:T(8,128)}) fusion(bf16[1024,4,32]{0,2,1:T(8,128)(2,1)S(1)} %get-tuple-element.258, bf16[8,1024,32]{1,2,0:T(8,128)(2,1)} %get-tuple-element.257, s32[]{:T(128)S(6)} %select_n.18, f32[4,1024,1024]{2,1,0:T(8,128)S(1)} %fusion.15, pred[1024,1024]{0,1:T(8,128)(4,1)} %broadcast_compare_fusion), kind=kOutput, calls=%fused_computation.67 | convolution fusion | flops 285208576 | bytes 34947076 | tf_op jit(solution)/shard_map/while/body/eval_jaxpr/cond/branch_1_fun/qhd,kd->hqk/dot_general | solution.py:96
  197.1 9.2 %fusion.5 = f32[4,1024]{1,0:T(4,128)S(1)} fusion(f32[4,1024,1024]{1,2,0:T(8,128)} %get-tuple-element.389, f32[4,1024]{1,0:T(4,128)S(1)} %max.5, pred[1024,1024]{0,1:T(8,128)(4,1)} %broadcast_compare_fusion), kind=kLoop, calls=%fused_computation.6 | loop fusion | flops 12578816 | bytes 17858560 | tf_op jit(solution)/shard_map/while/body/eval_jaxpr/cond/branch_1_fun/reduce_sum | solution.py:106
  206.3 8.8 %fusion.9 = f32[4,1024,64]{1,2,0:T(8,128)} fusion(f32[4,1024,1024]{1,2,0:T(8,128)} %get-tuple-element.389, f32[4,1024]{1,0:T(4,128)S(1)} %max.5, pred[1024,1024]{0,1:T(8,128)(4,1)S(1)} %copy-done.2, f32[4,1024,64]{1,2,0:T(8,128)} %get-tuple-element.260, bf16[1024,4,128]{0,2,1:T(8,128)(2,1)S(1)} %bitcast.45, f32[4,1024]{1,0:T(4,128)S(1)} %get-tuple-element.387), kind=kOutput, calls=%fused_computation.11 | convolution fusion | flops 549978112 | bytes 20480000 | tf_op jit(solution)/shard_map/while/body/eval_jaxpr/cond/branch_1_fun/hqk,khd->hqd/dot_general | solution.py:107
  216.2 36.1 %conditional.3 = ((f32[4,1024]{1,0:T(4,128)S(1)}, f32[4,1024]{1,0:T(4,128)S(1)}, f32[4,1024,64]{1,2,0:T(8,128)})) conditional(s32[]{:T(128)} %convert_element_type.106, (f32[4,1024]{1,0:T(4,128)S(1)}, f32[4,1024]{1,0:T(4,128)S(1)}, f32[4,1024,64]{1,2,0:T(8,128)}) %tuple.62, (s32[]{:T(128)}, s32[]{:T(128)}, s32[]{:T(128)}, ...), branch_computations={%region_4.4_spmd, %region_5.7_spmd} | conditional | flops 1923098624 | bytes 107565224 | solution.py:115
  218.0 1.7 broadcast_compare_fusion
  219.7 2.1 convolution_convert_fusion
  222.8 2.4 fusion.15
  225.2 9.2 %fusion.40 = (f32[4,1024]{1,0:T(4,128)S(1)}, f32[4,1024,1024]{1,2,0:T(8,128)}) fusion(bf16[1024,4,32]{0,2,1:T(8,128)(2,1)S(1)} %get-tuple-element.258, bf16[8,1024,32]{1,2,0:T(8,128)(2,1)} %get-tuple-element.257, s32[]{:T(128)S(6)} %select_n.18, f32[4,1024,1024]{2,1,0:T(8,128)S(1)} %fusion.15, pred[1024,1024]{0,1:T(8,128)(4,1)} %broadcast_compare_fusion), kind=kOutput, calls=%fused_computation.67 | convolution fusion | flops 285208576 | bytes 34947076 | tf_op jit(solution)/shard_map/while/body/eval_jaxpr/cond/branch_1_fun/qhd,kd->hqk/dot_general | solution.py:96
  234.3 9.2 %fusion.5 = f32[4,1024]{1,0:T(4,128)S(1)} fusion(f32[4,1024,1024]{1,2,0:T(8,128)} %get-tuple-element.389, f32[4,1024]{1,0:T(4,128)S(1)} %max.5, pred[1024,1024]{0,1:T(8,128)(4,1)} %broadcast_compare_fusion), kind=kLoop, calls=%fused_computation.6 | loop fusion | flops 12578816 | bytes 17858560 | tf_op jit(solution)/shard_map/while/body/eval_jaxpr/cond/branch_1_fun/reduce_sum | solution.py:106
  243.5 8.8 %fusion.9 = f32[4,1024,64]{1,2,0:T(8,128)} fusion(f32[4,1024,1024]{1,2,0:T(8,128)} %get-tuple-element.389, f32[4,1024]{1,0:T(4,128)S(1)} %max.5, pred[1024,1024]{0,1:T(8,128)(4,1)S(1)} %copy-done.2, f32[4,1024,64]{1,2,0:T(8,128)} %get-tuple-element.260, bf16[1024,4,128]{0,2,1:T(8,128)(2,1)S(1)} %bitcast.45, f32[4,1024]{1,0:T(4,128)S(1)} %get-tuple-element.387), kind=kOutput, calls=%fused_computation.11 | convolution fusion | flops 549978112 | bytes 20480000 | tf_op jit(solution)/shard_map/while/body/eval_jaxpr/cond/branch_1_fun/hqk,khd->hqd/dot_general | solution.py:107
  253.5 36.1 %conditional.3 = ((f32[4,1024]{1,0:T(4,128)S(1)}, f32[4,1024]{1,0:T(4,128)S(1)}, f32[4,1024,64]{1,2,0:T(8,128)})) conditional(s32[]{:T(128)} %convert_element_type.106, (f32[4,1024]{1,0:T(4,128)S(1)}, f32[4,1024]{1,0:T(4,128)S(1)}, f32[4,1024,64]{1,2,0:T(8,128)}) %tuple.62, (s32[]{:T(128)}, s32[]{:T(128)}, s32[]{:T(128)}, ...), branch_computations={%region_4.4_spmd, %region_5.7_spmd} | conditional | flops 1923098624 | bytes 107565224 | solution.py:115
  255.2 1.7 broadcast_compare_fusion
  256.9 2.1 convolution_convert_fusion
  260.0 2.4 fusion.15
  262.4 9.2 %fusion.40 = (f32[4,1024]{1,0:T(4,128)S(1)}, f32[4,1024,1024]{1,2,0:T(8,128)}) fusion(bf16[1024,4,32]{0,2,1:T(8,128)(2,1)S(1)} %get-tuple-element.258, bf16[8,1024,32]{1,2,0:T(8,128)(2,1)} %get-tuple-element.257, s32[]{:T(128)S(6)} %select_n.18, f32[4,1024,1024]{2,1,0:T(8,128)S(1)} %fusion.15, pred[1024,1024]{0,1:T(8,128)(4,1)} %broadcast_compare_fusion), kind=kOutput, calls=%fused_computation.67 | convolution fusion | flops 285208576 | bytes 34947076 | tf_op jit(solution)/shard_map/while/body/eval_jaxpr/cond/branch_1_fun/qhd,kd->hqk/dot_general | solution.py:96
  271.6 9.2 %fusion.5 = f32[4,1024]{1,0:T(4,128)S(1)} fusion(f32[4,1024,1024]{1,2,0:T(8,128)} %get-tuple-element.389, f32[4,1024]{1,0:T(4,128)S(1)} %max.5, pred[1024,1024]{0,1:T(8,128)(4,1)} %broadcast_compare_fusion), kind=kLoop, calls=%fused_computation.6 | loop fusion | flops 12578816 | bytes 17858560 | tf_op jit(solution)/shard_map/while/body/eval_jaxpr/cond/branch_1_fun/reduce_sum | solution.py:106
  280.8 8.8 %fusion.9 = f32[4,1024,64]{1,2,0:T(8,128)} fusion(f32[4,1024,1024]{1,2,0:T(8,128)} %get-tuple-element.389, f32[4,1024]{1,0:T(4,128)S(1)} %max.5, pred[1024,1024]{0,1:T(8,128)(4,1)S(1)} %copy-done.2, f32[4,1024,64]{1,2,0:T(8,128)} %get-tuple-element.260, bf16[1024,4,128]{0,2,1:T(8,128)(2,1)S(1)} %bitcast.45, f32[4,1024]{1,0:T(4,128)S(1)} %get-tuple-element.387), kind=kOutput, calls=%fused_computation.11 | convolution fusion | flops 549978112 | bytes 20480000 | tf_op jit(solution)/shard_map/while/body/eval_jaxpr/cond/branch_1_fun/hqk,khd->hqd/dot_general | solution.py:107
  290.7 36.1 %conditional.3 = ((f32[4,1024]{1,0:T(4,128)S(1)}, f32[4,1024]{1,0:T(4,128)S(1)}, f32[4,1024,64]{1,2,0:T(8,128)})) conditional(s32[]{:T(128)} %convert_element_type.106, (f32[4,1024]{1,0:T(4,128)S(1)}, f32[4,1024]{1,0:T(4,128)S(1)}, f32[4,1024,64]{1,2,0:T(8,128)}) %tuple.62, (s32[]{:T(128)}, s32[]{:T(128)}, s32[]{:T(128)}, ...), branch_computations={%region_4.4_spmd, %region_5.7_spmd} | conditional | flops 1923098624 | bytes 107565224 | solution.py:115
  294.1 2.1 convolution_convert_fusion
  297.2 2.4 fusion.15
  299.6 9.2 %fusion.40 = (f32[4,1024]{1,0:T(4,128)S(1)}, f32[4,1024,1024]{1,2,0:T(8,128)}) fusion(bf16[1024,4,32]{0,2,1:T(8,128)(2,1)S(1)} %get-tuple-element.258, bf16[8,1024,32]{1,2,0:T(8,128)(2,1)} %get-tuple-element.257, s32[]{:T(128)S(6)} %select_n.18, f32[4,1024,1024]{2,1,0:T(8,128)S(1)} %fusion.15, pred[1024,1024]{0,1:T(8,128)(4,1)} %broadcast_compare_fusion), kind=kOutput, calls=%fused_computation.67 | convolution fusion | flops 285208576 | bytes 34947076 | tf_op jit(solution)/shard_map/while/body/eval_jaxpr/cond/branch_1_fun/qhd,kd->hqk/dot_general | solution.py:96
  308.8 9.2 %fusion.5 = f32[4,1024]{1,0:T(4,128)S(1)} fusion(f32[4,1024,1024]{1,2,0:T(8,128)} %get-tuple-element.389, f32[4,1024]{1,0:T(4,128)S(1)} %max.5, pred[1024,1024]{0,1:T(8,128)(4,1)} %broadcast_compare_fusion), kind=kLoop, calls=%fused_computation.6 | loop fusion | flops 12578816 | bytes 17858560 | tf_op jit(solution)/shard_map/while/body/eval_jaxpr/cond/branch_1_fun/reduce_sum | solution.py:106
  318.0 8.8 %fusion.9 = f32[4,1024,64]{1,2,0:T(8,128)} fusion(f32[4,1024,1024]{1,2,0:T(8,128)} %get-tuple-element.389, f32[4,1024]{1,0:T(4,128)S(1)} %max.5, pred[1024,1024]{0,1:T(8,128)(4,1)S(1)} %copy-done.2, f32[4,1024,64]{1,2,0:T(8,128)} %get-tuple-element.260, bf16[1024,4,128]{0,2,1:T(8,128)(2,1)S(1)} %bitcast.45, f32[4,1024]{1,0:T(4,128)S(1)} %get-tuple-element.387), kind=kOutput, calls=%fused_computation.11 | convolution fusion | flops 549978112 | bytes 20480000 | tf_op jit(solution)/shard_map/while/body/eval_jaxpr/cond/branch_1_fun/hqk,khd->hqd/dot_general | solution.py:107
  327.9 36.1 %conditional.3 = ((f32[4,1024]{1,0:T(4,128)S(1)}, f32[4,1024]{1,0:T(4,128)S(1)}, f32[4,1024,64]{1,2,0:T(8,128)})) conditional(s32[]{:T(128)} %convert_element_type.106, (f32[4,1024]{1,0:T(4,128)S(1)}, f32[4,1024]{1,0:T(4,128)S(1)}, f32[4,1024,64]{1,2,0:T(8,128)}) %tuple.62, (s32[]{:T(128)}, s32[]{:T(128)}, s32[]{:T(128)}, ...), branch_computations={%region_4.4_spmd, %region_5.7_spmd} | conditional | flops 1923098624 | bytes 107565224 | solution.py:115
  331.3 2.1 convolution_convert_fusion
  334.4 2.4 fusion.15
  336.8 9.2 %fusion.40 = (f32[4,1024]{1,0:T(4,128)S(1)}, f32[4,1024,1024]{1,2,0:T(8,128)}) fusion(bf16[1024,4,32]{0,2,1:T(8,128)(2,1)S(1)} %get-tuple-element.258, bf16[8,1024,32]{1,2,0:T(8,128)(2,1)} %get-tuple-element.257, s32[]{:T(128)S(6)} %select_n.18, f32[4,1024,1024]{2,1,0:T(8,128)S(1)} %fusion.15, pred[1024,1024]{0,1:T(8,128)(4,1)} %broadcast_compare_fusion), kind=kOutput, calls=%fused_computation.67 | convolution fusion | flops 285208576 | bytes 34947076 | tf_op jit(solution)/shard_map/while/body/eval_jaxpr/cond/branch_1_fun/qhd,kd->hqk/dot_general | solution.py:96
  346.0 9.2 %fusion.5 = f32[4,1024]{1,0:T(4,128)S(1)} fusion(f32[4,1024,1024]{1,2,0:T(8,128)} %get-tuple-element.389, f32[4,1024]{1,0:T(4,128)S(1)} %max.5, pred[1024,1024]{0,1:T(8,128)(4,1)} %broadcast_compare_fusion), kind=kLoop, calls=%fused_computation.6 | loop fusion | flops 12578816 | bytes 17858560 | tf_op jit(solution)/shard_map/while/body/eval_jaxpr/cond/branch_1_fun/reduce_sum | solution.py:106
  355.2 8.8 %fusion.9 = f32[4,1024,64]{1,2,0:T(8,128)} fusion(f32[4,1024,1024]{1,2,0:T(8,128)} %get-tuple-element.389, f32[4,1024]{1,0:T(4,128)S(1)} %max.5, pred[1024,1024]{0,1:T(8,128)(4,1)S(1)} %copy-done.2, f32[4,1024,64]{1,2,0:T(8,128)} %get-tuple-element.260, bf16[1024,4,128]{0,2,1:T(8,128)(2,1)S(1)} %bitcast.45, f32[4,1024]{1,0:T(4,128)S(1)} %get-tuple-element.387), kind=kOutput, calls=%fused_computation.11 | convolution fusion | flops 549978112 | bytes 20480000 | tf_op jit(solution)/shard_map/while/body/eval_jaxpr/cond/branch_1_fun/hqk,khd->hqd/dot_general | solution.py:107
  365.1 36.1 %conditional.3 = ((f32[4,1024]{1,0:T(4,128)S(1)}, f32[4,1024]{1,0:T(4,128)S(1)}, f32[4,1024,64]{1,2,0:T(8,128)})) conditional(s32[]{:T(128)} %convert_element_type.106, (f32[4,1024]{1,0:T(4,128)S(1)}, f32[4,1024]{1,0:T(4,128)S(1)}, f32[4,1024,64]{1,2,0:T(8,128)}) %tuple.62, (s32[]{:T(128)}, s32[]{:T(128)}, s32[]{:T(128)}, ...), branch_computations={%region_4.4_spmd, %region_5.7_spmd} | conditional | flops 1923098624 | bytes 107565224 | solution.py:115
  368.5 2.1 convolution_convert_fusion
  371.6 2.4 fusion.15
  374.0 9.2 %fusion.40 = (f32[4,1024]{1,0:T(4,128)S(1)}, f32[4,1024,1024]{1,2,0:T(8,128)}) fusion(bf16[1024,4,32]{0,2,1:T(8,128)(2,1)S(1)} %get-tuple-element.258, bf16[8,1024,32]{1,2,0:T(8,128)(2,1)} %get-tuple-element.257, s32[]{:T(128)S(6)} %select_n.18, f32[4,1024,1024]{2,1,0:T(8,128)S(1)} %fusion.15, pred[1024,1024]{0,1:T(8,128)(4,1)} %broadcast_compare_fusion), kind=kOutput, calls=%fused_computation.67 | convolution fusion | flops 285208576 | bytes 34947076 | tf_op jit(solution)/shard_map/while/body/eval_jaxpr/cond/branch_1_fun/qhd,kd->hqk/dot_general | solution.py:96
  383.2 9.2 %fusion.5 = f32[4,1024]{1,0:T(4,128)S(1)} fusion(f32[4,1024,1024]{1,2,0:T(8,128)} %get-tuple-element.389, f32[4,1024]{1,0:T(4,128)S(1)} %max.5, pred[1024,1024]{0,1:T(8,128)(4,1)} %broadcast_compare_fusion), kind=kLoop, calls=%fused_computation.6 | loop fusion | flops 12578816 | bytes 17858560 | tf_op jit(solution)/shard_map/while/body/eval_jaxpr/cond/branch_1_fun/reduce_sum | solution.py:106
  392.4 8.8 %fusion.9 = f32[4,1024,64]{1,2,0:T(8,128)} fusion(f32[4,1024,1024]{1,2,0:T(8,128)} %get-tuple-element.389, f32[4,1024]{1,0:T(4,128)S(1)} %max.5, pred[1024,1024]{0,1:T(8,128)(4,1)S(1)} %copy-done.2, f32[4,1024,64]{1,2,0:T(8,128)} %get-tuple-element.260, bf16[1024,4,128]{0,2,1:T(8,128)(2,1)S(1)} %bitcast.45, f32[4,1024]{1,0:T(4,128)S(1)} %get-tuple-element.387), kind=kOutput, calls=%fused_computation.11 | convolution fusion | flops 549978112 | bytes 20480000 | tf_op jit(solution)/shard_map/while/body/eval_jaxpr/cond/branch_1_fun/hqk,khd->hqd/dot_general | solution.py:107
  402.3 36.1 %conditional.3 = ((f32[4,1024]{1,0:T(4,128)S(1)}, f32[4,1024]{1,0:T(4,128)S(1)}, f32[4,1024,64]{1,2,0:T(8,128)})) conditional(s32[]{:T(128)} %convert_element_type.106, (f32[4,1024]{1,0:T(4,128)S(1)}, f32[4,1024]{1,0:T(4,128)S(1)}, f32[4,1024,64]{1,2,0:T(8,128)}) %tuple.62, (s32[]{:T(128)}, s32[]{:T(128)}, s32[]{:T(128)}, ...), branch_computations={%region_4.4_spmd, %region_5.7_spmd} | conditional | flops 1923098624 | bytes 107565224 | solution.py:115
  404.0 1.7 broadcast_compare_fusion
  405.8 2.1 convolution_convert_fusion
  408.8 2.4 fusion.15
  411.2 9.2 %fusion.40 = (f32[4,1024]{1,0:T(4,128)S(1)}, f32[4,1024,1024]{1,2,0:T(8,128)}) fusion(bf16[1024,4,32]{0,2,1:T(8,128)(2,1)S(1)} %get-tuple-element.258, bf16[8,1024,32]{1,2,0:T(8,128)(2,1)} %get-tuple-element.257, s32[]{:T(128)S(6)} %select_n.18, f32[4,1024,1024]{2,1,0:T(8,128)S(1)} %fusion.15, pred[1024,1024]{0,1:T(8,128)(4,1)} %broadcast_compare_fusion), kind=kOutput, calls=%fused_computation.67 | convolution fusion | flops 285208576 | bytes 34947076 | tf_op jit(solution)/shard_map/while/body/eval_jaxpr/cond/branch_1_fun/qhd,kd->hqk/dot_general | solution.py:96
  420.4 9.2 %fusion.5 = f32[4,1024]{1,0:T(4,128)S(1)} fusion(f32[4,1024,1024]{1,2,0:T(8,128)} %get-tuple-element.389, f32[4,1024]{1,0:T(4,128)S(1)} %max.5, pred[1024,1024]{0,1:T(8,128)(4,1)} %broadcast_compare_fusion), kind=kLoop, calls=%fused_computation.6 | loop fusion | flops 12578816 | bytes 17858560 | tf_op jit(solution)/shard_map/while/body/eval_jaxpr/cond/branch_1_fun/reduce_sum | solution.py:106
  429.6 8.8 %fusion.9 = f32[4,1024,64]{1,2,0:T(8,128)} fusion(f32[4,1024,1024]{1,2,0:T(8,128)} %get-tuple-element.389, f32[4,1024]{1,0:T(4,128)S(1)} %max.5, pred[1024,1024]{0,1:T(8,128)(4,1)S(1)} %copy-done.2, f32[4,1024,64]{1,2,0:T(8,128)} %get-tuple-element.260, bf16[1024,4,128]{0,2,1:T(8,128)(2,1)S(1)} %bitcast.45, f32[4,1024]{1,0:T(4,128)S(1)} %get-tuple-element.387), kind=kOutput, calls=%fused_computation.11 | convolution fusion | flops 549978112 | bytes 20480000 | tf_op jit(solution)/shard_map/while/body/eval_jaxpr/cond/branch_1_fun/hqk,khd->hqd/dot_general | solution.py:107
  439.5 36.1 %conditional.3 = ((f32[4,1024]{1,0:T(4,128)S(1)}, f32[4,1024]{1,0:T(4,128)S(1)}, f32[4,1024,64]{1,2,0:T(8,128)})) conditional(s32[]{:T(128)} %convert_element_type.106, (f32[4,1024]{1,0:T(4,128)S(1)}, f32[4,1024]{1,0:T(4,128)S(1)}, f32[4,1024,64]{1,2,0:T(8,128)}) %tuple.62, (s32[]{:T(128)}, s32[]{:T(128)}, s32[]{:T(128)}, ...), branch_computations={%region_4.4_spmd, %region_5.7_spmd} | conditional | flops 1923098624 | bytes 107565224 | solution.py:115
  443.0 2.1 convolution_convert_fusion
  446.0 2.4 fusion.15
  448.4 9.2 %fusion.40 = (f32[4,1024]{1,0:T(4,128)S(1)}, f32[4,1024,1024]{1,2,0:T(8,128)}) fusion(bf16[1024,4,32]{0,2,1:T(8,128)(2,1)S(1)} %get-tuple-element.258, bf16[8,1024,32]{1,2,0:T(8,128)(2,1)} %get-tuple-element.257, s32[]{:T(128)S(6)} %select_n.18, f32[4,1024,1024]{2,1,0:T(8,128)S(1)} %fusion.15, pred[1024,1024]{0,1:T(8,128)(4,1)} %broadcast_compare_fusion), kind=kOutput, calls=%fused_computation.67 | convolution fusion | flops 285208576 | bytes 34947076 | tf_op jit(solution)/shard_map/while/body/eval_jaxpr/cond/branch_1_fun/qhd,kd->hqk/dot_general | solution.py:96
  457.6 9.2 %fusion.5 = f32[4,1024]{1,0:T(4,128)S(1)} fusion(f32[4,1024,1024]{1,2,0:T(8,128)} %get-tuple-element.389, f32[4,1024]{1,0:T(4,128)S(1)} %max.5, pred[1024,1024]{0,1:T(8,128)(4,1)} %broadcast_compare_fusion), kind=kLoop, calls=%fused_computation.6 | loop fusion | flops 12578816 | bytes 17858560 | tf_op jit(solution)/shard_map/while/body/eval_jaxpr/cond/branch_1_fun/reduce_sum | solution.py:106
  466.8 8.8 %fusion.9 = f32[4,1024,64]{1,2,0:T(8,128)} fusion(f32[4,1024,1024]{1,2,0:T(8,128)} %get-tuple-element.389, f32[4,1024]{1,0:T(4,128)S(1)} %max.5, pred[1024,1024]{0,1:T(8,128)(4,1)S(1)} %copy-done.2, f32[4,1024,64]{1,2,0:T(8,128)} %get-tuple-element.260, bf16[1024,4,128]{0,2,1:T(8,128)(2,1)S(1)} %bitcast.45, f32[4,1024]{1,0:T(4,128)S(1)} %get-tuple-element.387), kind=kOutput, calls=%fused_computation.11 | convolution fusion | flops 549978112 | bytes 20480000 | tf_op jit(solution)/shard_map/while/body/eval_jaxpr/cond/branch_1_fun/hqk,khd->hqd/dot_general | solution.py:107
  477.4 11.4 %all_to_all.16 = bf16[4,256,256]{1,2,0:T(8,128)(2,1)S(1)} all-to-all(bf16[4,256,256]{1,2,0:T(8,128)(2,1)S(1)} %copy.21), channel_id=1, replica_groups=mesh['sp'=8,'tp'=4] {'tp'}, dimensions={0} | all-to-all | bytes 1048576 | tf_op jit(solution)/shard_map/all_to_all | solution.py:139
  488.7 5.9 %multiply_reduce_fusion = (f32[256]{0:T(256)S(1)}, f32[256,4096]{1,0:T(8,128)S(1)}) fusion(bf16[256,1024]{0,1:T(8,128)(2,1)S(1)} %bitcast.48, bf16[1024,4096]{1,0:T(8,128)(2,1)} %param.24), kind=kOutput, calls=%fused_computation.32 | convolution fusion | flops 2149580544 | bytes 13108224 | tf_op jit(solution)/shard_map/dot_general | solution.py:140
  494.7 1.9 multiply_convert_fusion
  (147 shorter events, 26.6 us)
Async XLA Ops:
  6.5 65.0 %copy-start = (bf16[768,384]{1,0:T(8,128)(2,1)S(1)}, bf16[768,384]{1,0:T(8,128)(2,1)}, u32[]{:S(2)}) copy-start(bf16[768,384]{1,0:T(8,128)(2,1)} %param.22) | copy-start | bytes 1769476
  6.5 25.2 %all-gather.4.cloned.1.call-start = ((), (), s32[]{:S(2)}) async-start(), calls=%async_computation.1 | async-start | bytes 1310720 | tf_op jit(solution)/shard_map/all_gather | solution.py:65
  8.7 4.4 copy-start.8
  8.7 5.3 %copy-start.5 = (bf16[256,4096]{1,0:T(8,128)(2,1)S(1)}, bf16[256,4096]{1,0:T(8,128)(2,1)}, u32[]{:S(2)}) copy-start(bf16[256,4096]{1,0:T(8,128)(2,1)} %param.15) | copy-start | bytes 6291460
  8.7 5.3 %copy-start.10 = (f32[4096]{0:T(1024)S(1)}, f32[4096]{0:T(1024)}, u32[]{:S(2)}) copy-start(f32[4096]{0:T(1024)} %param.16) | copy-start | bytes 49156
  14.0 4.8 copy-start.7
  14.0 17.9 %copy-start.9 = (bf16[4096,32]{0,1:T(8,128)(2,1)S(1)}, bf16[4096,32]{0,1:T(8,128)(2,1)}, u32[]{:S(2)}) copy-start(bf16[4096,32]{0,1:T(8,128)(2,1)} %param.19) | copy-start | bytes 786436
  14.0 57.5 %all-gather.8.cloned.1.call-start = ((), (), s32[]{:S(2)}) async-start(), calls=%async_computation.3 | async-start | bytes 1966080 | tf_op jit(solution)/shard_map/all_gather | solution.py:64
  19.7 157.1 %all-gather.6.cloned.1.call-start = ((), (), s32[]{:S(2)}) async-start(), calls=%async_computation.2 | async-start | bytes 9437184 | tf_op jit(solution)/shard_map/all_gather | solution.py:124
  184.6 1.0 copy-start.3
  197.1 9.2 %copy-start.2 = (pred[1024,1024]{0,1:T(8,128)(4,1)S(1)}, pred[1024,1024]{0,1:T(8,128)(4,1)}, u32[]{:S(2)}) copy-start(pred[1024,1024]{0,1:T(8,128)(4,1)} %broadcast_compare_fusion) | copy-start | bytes 3145732 | tf_op jit(solution)/shard_map/while/body/eval_jaxpr/cond
  197.1 9.2 %copy-start.4 = (bf16[1024,512]{0,1:T(8,128)(2,1)S(1)}, bf16[1024,512]{0,1:T(8,128)(2,1)}, u32[]{:S(2)}) copy-start(bf16[1024,512]{0,1:T(8,128)(2,1)} %copy-done.3) | copy-start | bytes 3145732 | tf_op jit(solution)/shard_map/while/body/eval_jaxpr/cond
  221.8 1.0 copy-start.3
  234.3 9.2 %copy-start.2 = (pred[1024,1024]{0,1:T(8,128)(4,1)S(1)}, pred[1024,1024]{0,1:T(8,128)(4,1)}, u32[]{:S(2)}) copy-start(pred[1024,1024]{0,1:T(8,128)(4,1)} %broadcast_compare_fusion) | copy-start | bytes 3145732 | tf_op jit(solution)/shard_map/while/body/eval_jaxpr/cond
  234.3 9.2 %copy-start.4 = (bf16[1024,512]{0,1:T(8,128)(2,1)S(1)}, bf16[1024,512]{0,1:T(8,128)(2,1)}, u32[]{:S(2)}) copy-start(bf16[1024,512]{0,1:T(8,128)(2,1)} %copy-done.3) | copy-start | bytes 3145732 | tf_op jit(solution)/shard_map/while/body/eval_jaxpr/cond
  259.0 1.0 copy-start.3
  271.5 9.2 %copy-start.2 = (pred[1024,1024]{0,1:T(8,128)(4,1)S(1)}, pred[1024,1024]{0,1:T(8,128)(4,1)}, u32[]{:S(2)}) copy-start(pred[1024,1024]{0,1:T(8,128)(4,1)} %broadcast_compare_fusion) | copy-start | bytes 3145732 | tf_op jit(solution)/shard_map/while/body/eval_jaxpr/cond
  271.5 9.2 %copy-start.4 = (bf16[1024,512]{0,1:T(8,128)(2,1)S(1)}, bf16[1024,512]{0,1:T(8,128)(2,1)}, u32[]{:S(2)}) copy-start(bf16[1024,512]{0,1:T(8,128)(2,1)} %copy-done.3) | copy-start | bytes 3145732 | tf_op jit(solution)/shard_map/while/body/eval_jaxpr/cond
  296.2 1.0 copy-start.3
  308.7 9.2 %copy-start.2 = (pred[1024,1024]{0,1:T(8,128)(4,1)S(1)}, pred[1024,1024]{0,1:T(8,128)(4,1)}, u32[]{:S(2)}) copy-start(pred[1024,1024]{0,1:T(8,128)(4,1)} %broadcast_compare_fusion) | copy-start | bytes 3145732 | tf_op jit(solution)/shard_map/while/body/eval_jaxpr/cond
  308.8 9.2 %copy-start.4 = (bf16[1024,512]{0,1:T(8,128)(2,1)S(1)}, bf16[1024,512]{0,1:T(8,128)(2,1)}, u32[]{:S(2)}) copy-start(bf16[1024,512]{0,1:T(8,128)(2,1)} %copy-done.3) | copy-start | bytes 3145732 | tf_op jit(solution)/shard_map/while/body/eval_jaxpr/cond
  333.4 1.0 copy-start.3
  346.0 9.2 %copy-start.2 = (pred[1024,1024]{0,1:T(8,128)(4,1)S(1)}, pred[1024,1024]{0,1:T(8,128)(4,1)}, u32[]{:S(2)}) copy-start(pred[1024,1024]{0,1:T(8,128)(4,1)} %broadcast_compare_fusion) | copy-start | bytes 3145732 | tf_op jit(solution)/shard_map/while/body/eval_jaxpr/cond
  346.0 9.2 %copy-start.4 = (bf16[1024,512]{0,1:T(8,128)(2,1)S(1)}, bf16[1024,512]{0,1:T(8,128)(2,1)}, u32[]{:S(2)}) copy-start(bf16[1024,512]{0,1:T(8,128)(2,1)} %copy-done.3) | copy-start | bytes 3145732 | tf_op jit(solution)/shard_map/while/body/eval_jaxpr/cond
  370.7 1.0 copy-start.3
  383.2 9.2 %copy-start.2 = (pred[1024,1024]{0,1:T(8,128)(4,1)S(1)}, pred[1024,1024]{0,1:T(8,128)(4,1)}, u32[]{:S(2)}) copy-start(pred[1024,1024]{0,1:T(8,128)(4,1)} %broadcast_compare_fusion) | copy-start | bytes 3145732 | tf_op jit(solution)/shard_map/while/body/eval_jaxpr/cond
  383.2 9.2 %copy-start.4 = (bf16[1024,512]{0,1:T(8,128)(2,1)S(1)}, bf16[1024,512]{0,1:T(8,128)(2,1)}, u32[]{:S(2)}) copy-start(bf16[1024,512]{0,1:T(8,128)(2,1)} %copy-done.3) | copy-start | bytes 3145732 | tf_op jit(solution)/shard_map/while/body/eval_jaxpr/cond
  407.9 1.0 copy-start.3
  420.4 9.2 %copy-start.2 = (pred[1024,1024]{0,1:T(8,128)(4,1)S(1)}, pred[1024,1024]{0,1:T(8,128)(4,1)}, u32[]{:S(2)}) copy-start(pred[1024,1024]{0,1:T(8,128)(4,1)} %broadcast_compare_fusion) | copy-start | bytes 3145732 | tf_op jit(solution)/shard_map/while/body/eval_jaxpr/cond
  420.4 9.2 %copy-start.4 = (bf16[1024,512]{0,1:T(8,128)(2,1)S(1)}, bf16[1024,512]{0,1:T(8,128)(2,1)}, u32[]{:S(2)}) copy-start(bf16[1024,512]{0,1:T(8,128)(2,1)} %copy-done.3) | copy-start | bytes 3145732 | tf_op jit(solution)/shard_map/while/body/eval_jaxpr/cond
  445.1 1.0 copy-start.3
  457.6 9.2 %copy-start.2 = (pred[1024,1024]{0,1:T(8,128)(4,1)S(1)}, pred[1024,1024]{0,1:T(8,128)(4,1)}, u32[]{:S(2)}) copy-start(pred[1024,1024]{0,1:T(8,128)(4,1)} %broadcast_compare_fusion) | copy-start | bytes 3145732 | tf_op jit(solution)/shard_map/while/body/eval_jaxpr/cond
  457.6 9.2 %copy-start.4 = (bf16[1024,512]{0,1:T(8,128)(2,1)S(1)}, bf16[1024,512]{0,1:T(8,128)(2,1)}, u32[]{:S(2)}) copy-start(bf16[1024,512]{0,1:T(8,128)(2,1)} %copy-done.3) | copy-start | bytes 3145732 | tf_op jit(solution)/shard_map/while/body/eval_jaxpr/cond
  488.7 6.0 %copy-start.6 = (f32[4096]{0:T(1024)S(1)}, f32[4096]{0:T(1024)}, u32[]{:S(2)}) copy-start(f32[4096]{0:T(1024)} %param.25) | copy-start | bytes 49156
  488.7 7.9 %copy-start.1 = (bf16[768,384]{1,0:T(8,128)(2,1)S(1)}, bf16[768,384]{1,0:T(8,128)(2,1)}, u32[]{:S(2)}) copy-start(bf16[768,384]{1,0:T(8,128)(2,1)} %param.22) | copy-start | bytes 1769476
Sparse Core Ops, SparseCore 0:
  14.1 17.6 all-gather.3
  33.3 19.6 all-gather.7
  55.1 121.5 all-gather.5
where the time goes:
time: 504 us; the launch traced here: 503 us
  matrix products  197 us (39%)
  waiting for transfers between devices  115 us (23%)
  other arithmetic  94.9 us (19%)
  blocking collectives  48.9 us (10%)
  loops' own time  18.9 us (4%)
  local copies, waits for them, and re-layouts  14.8 us (3%)
  between operations  13.3 us (3%)
    all_gather x1, waiting for transfers between devices, local(): key_piece = lax.all_gather(kv_group, 'sp', axis=0, tiled=True)  103 us
    dot_general x8, matrix products, compute(): jnp.einsum('qhd,kd->hqk', query_rot, rot_rows, preferred_element_type=jnp...  73.2 us
    reduce_sum x8, other arithmetic, compute(): total_new = total * correction + jnp.sum(weights, axis=-1)  73.2 us
    dot_general x8, matrix products, compute(): jnp.einsum('hqk,khd->hqd', weights.astype(jnp.bfloat16), keys_values[...,...  70.1 us
    all_gather x1, blocking collectives, local(): rot_piece = lax.all_gather(rot_group, 'sp', axis=0, tiled=True)  32.3 us
    dot_general x8, matrix products, compute(): jnp.einsum('qhd,khd->hqk', query_nope, keys_values[..., :NOPE], preferred...  19 us
    dot_general x8, matrix products, compute(): jnp.dot(key_rows, kv_up, preferred_element_type=jnp.float32)  16.8 us
    another operation x8, loops' own time, attend_block(): lax.cond(block_first <= query_first + group_rows - 1, compute, lambda sta...  14.3 us
  transfers between devices with their start and end apart: 3, of which 2 were waited for; matrix products, arithmetic and copies ran while one was open for 2% of the time, Pallas kernels for 0%

commit v1 on v0

--- a/solution.py
+++ b/solution.py
@@ -121,8 +121,11 @@
         jnp.zeros((head_count, group_rows), jnp.float32),
         jnp.zeros((head_count, group_rows, VDIM), jnp.float32),
     )
-    key_piece = lax.all_gather(kv_group, "sp", axis=0, tiled=True)
-    rot_piece = lax.all_gather(rot_group, "sp", axis=0, tiled=True)
+    key_piece, rot_piece = jnp.split(
+        lax.all_gather(jnp.concatenate([kv_group, rot_group], axis=1), "sp", axis=0, tiled=True),
+        [kv_group.shape[1]],
+        axis=1,
+    )
     piece_rows = rot_piece.shape[0]
     block_count = piece_rows // group_rows
     key_blocks = key_piece.reshape((block_count, group_rows) + key_piece.shape[1:])

time: 504 us -> 547 us (1.085)
  waiting for transfers between devices: 115 us -> 171 us
  blocking collectives: 48.9 us -> 18.7 us
  local copies, waits for them, and re-layouts: 14.8 us -> 25.2 us
    all_gather x1, waiting for transfers between devices: 103 us -> 147 us  [local(): lax.all_gather(jnp.concatenate([kv_group, rot_group], axis=1), 'sp', axis...]
    all_gather x1 -> x0, blocking collectives: 32.3 us -> none  [local(): rot_piece = lax.all_gather(rot_group, 'sp', axis=0, tiled=True)]
    all_gather x1, waiting for transfers between devices: 0.02 us -> 18.8 us  [local(): lax.all_gather(q_lat, 'tp', axis=0, tiled=True)]
    split x0 -> x3, local copies, waits for them, and re-layouts: none -> 8.74 us  [local(): jnp.split(lax.all_gather(jnp.concatenate([kv_group, rot_group], axis=1),...]
    all_gather x1, waiting for transfers between devices: 12 us -> 4.79 us  [local(): lax.all_gather(kv_lat, 'tp', axis=0, tiled=True)]
  transfers between devices with their start and end apart: 3 -> 3, of which waited for: 2 -> 3; matrix products, arithmetic and copies ran while one was open for 2% -> 2% of each run, Pallas kernels for 0% -> 0%
where the time goes in v1:
time: 547 us; the launch traced here: 546 us
  matrix products  197 us (36%)
  waiting for transfers between devices  171 us (31%)
  other arithmetic  97.2 us (18%)
  local copies, waits for them, and re-layouts  25.2 us (5%)
  loops' own time  22.9 us (4%)
  blocking collectives  18.7 us (3%)
  between operations  13.3 us (2%)
    all_gather x1, waiting for transfers between devices, local(): lax.all_gather(jnp.concatenate([kv_group, rot_group], axis=1), 'sp', axis...  147 us
    reduce_sum x8, other arithmetic, compute(): total_new = total * correction + jnp.sum(weights, axis=-1)  73.2 us
    dot_general x8, matrix products, compute(): jnp.einsum('qhd,kd->hqk', query_rot, rot_rows, preferred_element_type=jnp...  73.2 us
    dot_general x8, matrix products, compute(): jnp.einsum('hqk,khd->hqd', weights.astype(jnp.bfloat16), keys_values[...,...  70 us
    dot_general x8, matrix products, compute(): jnp.einsum('qhd,khd->hqk', query_nope, keys_values[..., :NOPE], preferred...  19 us
    all_gather x1, waiting for transfers between devices, local(): lax.all_gather(q_lat, 'tp', axis=0, tiled=True)  18.8 us
    another operation x8, loops' own time, attend_block(): lax.cond(block_first <= query_first + group_rows - 1, compute, lambda sta...  17.2 us
    dot_general x8, matrix products, compute(): jnp.dot(key_rows, kv_up, preferred_element_type=jnp.float32)  16.8 us
  transfers between devices with their start and end apart: 3, of which 3 were waited for; matrix products, arithmetic and copies ran while one was open for 2% of the time, Pallas kernels for 0%

profile of v1, /device:TPU:26, one launch (start us, length us, event | category | flops | bytes accessed | tf_op | source)
XLA Modules:
  0.0 545.6 jit_solution(12571945991478774259)
XLA Ops:
  6.5 2.1 fusion.22
  8.7 4.4 multiply_reduce_fusion.2
  14.0 4.7 multiply_reduce_fusion.1
  20.9 7.2 %all_gather.13 = bf16[1024,32]{1,0:T(8,128)(2,1)S(1)} all-gather(bf16[256,32]{1,0:T(8,128)(2,1)S(1)} %copy.26), channel_id=1, replica_groups=mesh['sp'=8,'tp'=4] {'tp'}, dimensions={0}, use_global_device_ids=true | all-gather | bytes 81920 | tf_op jit(solution)/shard_map/all_gather | solution.py:66
  28.1 4.8 all-gather.4.cloned.1.call-done
  32.9 2.4 pad_maximum_fusion
  35.7 18.8 %all-gather.8.cloned.1.call-done = bf16[1024,768]{1,0:T(8,128)(2,1)} async-done(((bf16[256,768]{1,0:T(8,128)(2,1)}), bf16[1024,768]{1,0:T(8,128)(2,1)}) %all-gather.8.cloned.1.call-update) | async-done | bytes 1572880 | tf_op jit(solution)/shard_map/all_gather | solution.py:64
  54.4 2.2 fusion.41
  56.8 147.5 %all-gather.6.cloned.1.call-done = bf16[8192,544]{1,0:T(8,128)(2,1)} async-done(((bf16[1024,544]{1,0:T(8,128)(2,1)}), bf16[8192,544]{1,0:T(8,128)(2,1)}) %all-gather.6.cloned.1.call-update) | async-done | bytes 8912912 | tf_op jit(solution)/shard_map/all_gather | solution.py:125
  207.4 7.1 %split.8 = bf16[8192,512]{1,0:T(8,128)(2,1)} slice(bf16[8192,544]{1,0:T(8,128)(2,1)} %all-gather.6.cloned.1.call-done), slice={[0:8192], [0:512]} | slice | bytes 16777216 | tf_op jit(solution)/shard_map/split | solution.py:124
  215.7 302.4 %while.17 = (s32[]{:T(128)}, f32[4,1024]{1,0:T(4,128)S(1)}, f32[4,1024]{1,0:T(4,128)S(1)}, f32[4,1024,64]{1,2,0:T(8,128)}, s32[8]{0:T(128)S(1)}, /*index=5*/s32[...) while((s32[]{:T(128)}, f32[4,1024]{1,0:T(4,128)S(1)}, ...), condition=%wide.region_8.9_spmd.clone, body=%wide.region_3.8_spmd.clone.sunk | while | flops 1923098624 | bytes 107569616 | solution.py:138
  217.0 36.4 %conditional.3 = ((f32[4,1024]{1,0:T(4,128)S(1)}, f32[4,1024]{1,0:T(4,128)S(1)}, f32[4,1024,64]{1,2,0:T(8,128)})) conditional(s32[]{:T(128)} %convert_element_type.106, (f32[4,1024]{1,0:T(4,128)S(1)}, f32[4,1024]{1,0:T(4,128)S(1)}, f32[4,1024,64]{1,2,0:T(8,128)}) %tuple.62, (s32[]{:T(128)}, s32[]{:T(128)}, s32[]{:T(128)}, ...), branch_computations={%region_4.4_spmd, %region_5.7_spmd} | conditional | flops 1923098624 | bytes 107565224 | solution.py:115
  220.8 2.1 convolution_convert_fusion
  223.9 2.4 fusion.15
  226.3 9.2 %fusion.40 = (f32[4,1024]{1,0:T(4,128)S(1)}, f32[4,1024,1024]{1,2,0:T(8,128)}) fusion(bf16[1024,4,32]{0,2,1:T(8,128)(2,1)S(1)} %get-tuple-element.258, bf16[8,1024,32]{1,2,0:T(8,128)(2,1)} %get-tuple-element.257, s32[]{:T(128)S(6)} %select_n.18, f32[4,1024,1024]{2,1,0:T(8,128)S(1)} %fusion.15, pred[1024,1024]{0,1:T(8,128)(4,1)} %broadcast_compare_fusion), kind=kOutput, calls=%fused_computation.67 | convolution fusion | flops 285208576 | bytes 34947076 | tf_op jit(solution)/shard_map/while/body/eval_jaxpr/cond/branch_1_fun/qhd,kd->hqk/dot_general | solution.py:96
  235.5 9.2 %fusion.5 = f32[4,1024]{1,0:T(4,128)S(1)} fusion(f32[4,1024,1024]{1,2,0:T(8,128)} %get-tuple-element.389, f32[4,1024]{1,0:T(4,128)S(1)} %max.5, pred[1024,1024]{0,1:T(8,128)(4,1)} %broadcast_compare_fusion), kind=kLoop, calls=%fused_computation.6 | loop fusion | flops 12578816 | bytes 17858560 | tf_op jit(solution)/shard_map/while/body/eval_jaxpr/cond/branch_1_fun/reduce_sum | solution.py:106
  244.7 8.8 %fusion.9 = f32[4,1024,64]{1,2,0:T(8,128)} fusion(f32[4,1024,1024]{1,2,0:T(8,128)} %get-tuple-element.389, f32[4,1024]{1,0:T(4,128)S(1)} %max.5, pred[1024,1024]{0,1:T(8,128)(4,1)S(1)} %copy-done.2, f32[4,1024,64]{1,2,0:T(8,128)} %get-tuple-element.260, bf16[1024,4,128]{0,2,1:T(8,128)(2,1)S(1)} %bitcast.42, f32[4,1024]{1,0:T(4,128)S(1)} %get-tuple-element.387), kind=kOutput, calls=%fused_computation.11 | convolution fusion | flops 549978112 | bytes 20480000 | tf_op jit(solution)/shard_map/while/body/eval_jaxpr/cond/branch_1_fun/hqk,khd->hqd/dot_general | solution.py:107
  254.8 36.4 %conditional.3 = ((f32[4,1024]{1,0:T(4,128)S(1)}, f32[4,1024]{1,0:T(4,128)S(1)}, f32[4,1024,64]{1,2,0:T(8,128)})) conditional(s32[]{:T(128)} %convert_element_type.106, (f32[4,1024]{1,0:T(4,128)S(1)}, f32[4,1024]{1,0:T(4,128)S(1)}, f32[4,1024,64]{1,2,0:T(8,128)}) %tuple.62, (s32[]{:T(128)}, s32[]{:T(128)}, s32[]{:T(128)}, ...), branch_computations={%region_4.4_spmd, %region_5.7_spmd} | conditional | flops 1923098624 | bytes 107565224 | solution.py:115
  256.9 1.7 broadcast_compare_fusion
  258.6 2.1 convolution_convert_fusion
  261.7 2.4 fusion.15
  264.1 9.2 %fusion.40 = (f32[4,1024]{1,0:T(4,128)S(1)}, f32[4,1024,1024]{1,2,0:T(8,128)}) fusion(bf16[1024,4,32]{0,2,1:T(8,128)(2,1)S(1)} %get-tuple-element.258, bf16[8,1024,32]{1,2,0:T(8,128)(2,1)} %get-tuple-element.257, s32[]{:T(128)S(6)} %select_n.18, f32[4,1024,1024]{2,1,0:T(8,128)S(1)} %fusion.15, pred[1024,1024]{0,1:T(8,128)(4,1)} %broadcast_compare_fusion), kind=kOutput, calls=%fused_computation.67 | convolution fusion | flops 285208576 | bytes 34947076 | tf_op jit(solution)/shard_map/while/body/eval_jaxpr/cond/branch_1_fun/qhd,kd->hqk/dot_general | solution.py:96
  273.3 9.2 %fusion.5 = f32[4,1024]{1,0:T(4,128)S(1)} fusion(f32[4,1024,1024]{1,2,0:T(8,128)} %get-tuple-element.389, f32[4,1024]{1,0:T(4,128)S(1)} %max.5, pred[1024,1024]{0,1:T(8,128)(4,1)} %broadcast_compare_fusion), kind=kLoop, calls=%fused_computation.6 | loop fusion | flops 12578816 | bytes 17858560 | tf_op jit(solution)/shard_map/while/body/eval_jaxpr/cond/branch_1_fun/reduce_sum | solution.py:106
  282.5 8.8 %fusion.9 = f32[4,1024,64]{1,2,0:T(8,128)} fusion(f32[4,1024,1024]{1,2,0:T(8,128)} %get-tuple-element.389, f32[4,1024]{1,0:T(4,128)S(1)} %max.5, pred[1024,1024]{0,1:T(8,128)(4,1)S(1)} %copy-done.2, f32[4,1024,64]{1,2,0:T(8,128)} %get-tuple-element.260, bf16[1024,4,128]{0,2,1:T(8,128)(2,1)S(1)} %bitcast.42, f32[4,1024]{1,0:T(4,128)S(1)} %get-tuple-element.387), kind=kOutput, calls=%fused_computation.11 | convolution fusion | flops 549978112 | bytes 20480000 | tf_op jit(solution)/shard_map/while/body/eval_jaxpr/cond/branch_1_fun/hqk,khd->hqd/dot_general | solution.py:107
  292.6 36.4 %conditional.3 = ((f32[4,1024]{1,0:T(4,128)S(1)}, f32[4,1024]{1,0:T(4,128)S(1)}, f32[4,1024,64]{1,2,0:T(8,128)})) conditional(s32[]{:T(128)} %convert_element_type.106, (f32[4,1024]{1,0:T(4,128)S(1)}, f32[4,1024]{1,0:T(4,128)S(1)}, f32[4,1024,64]{1,2,0:T(8,128)}) %tuple.62, (s32[]{:T(128)}, s32[]{:T(128)}, s32[]{:T(128)}, ...), branch_computations={%region_4.4_spmd, %region_5.7_spmd} | conditional | flops 1923098624 | bytes 107565224 | solution.py:115
  296.4 2.1 convolution_convert_fusion
  299.5 2.4 fusion.15
  301.9 9.2 %fusion.40 = (f32[4,1024]{1,0:T(4,128)S(1)}, f32[4,1024,1024]{1,2,0:T(8,128)}) fusion(bf16[1024,4,32]{0,2,1:T(8,128)(2,1)S(1)} %get-tuple-element.258, bf16[8,1024,32]{1,2,0:T(8,128)(2,1)} %get-tuple-element.257, s32[]{:T(128)S(6)} %select_n.18, f32[4,1024,1024]{2,1,0:T(8,128)S(1)} %fusion.15, pred[1024,1024]{0,1:T(8,128)(4,1)} %broadcast_compare_fusion), kind=kOutput, calls=%fused_computation.67 | convolution fusion | flops 285208576 | bytes 34947076 | tf_op jit(solution)/shard_map/while/body/eval_jaxpr/cond/branch_1_fun/qhd,kd->hqk/dot_general | solution.py:96
  311.1 9.2 %fusion.5 = f32[4,1024]{1,0:T(4,128)S(1)} fusion(f32[4,1024,1024]{1,2,0:T(8,128)} %get-tuple-element.389, f32[4,1024]{1,0:T(4,128)S(1)} %max.5, pred[1024,1024]{0,1:T(8,128)(4,1)} %broadcast_compare_fusion), kind=kLoop, calls=%fused_computation.6 | loop fusion | flops 12578816 | bytes 17858560 | tf_op jit(solution)/shard_map/while/body/eval_jaxpr/cond/branch_1_fun/reduce_sum | solution.py:106
  320.3 8.8 %fusion.9 = f32[4,1024,64]{1,2,0:T(8,128)} fusion(f32[4,1024,1024]{1,2,0:T(8,128)} %get-tuple-element.389, f32[4,1024]{1,0:T(4,128)S(1)} %max.5, pred[1024,1024]{0,1:T(8,128)(4,1)S(1)} %copy-done.2, f32[4,1024,64]{1,2,0:T(8,128)} %get-tuple-element.260, bf16[1024,4,128]{0,2,1:T(8,128)(2,1)S(1)} %bitcast.42, f32[4,1024]{1,0:T(4,128)S(1)} %get-tuple-element.387), kind=kOutput, calls=%fused_computation.11 | convolution fusion | flops 549978112 | bytes 20480000 | tf_op jit(solution)/shard_map/while/body/eval_jaxpr/cond/branch_1_fun/hqk,khd->hqd/dot_general | solution.py:107
  330.4 36.4 %conditional.3 = ((f32[4,1024]{1,0:T(4,128)S(1)}, f32[4,1024]{1,0:T(4,128)S(1)}, f32[4,1024,64]{1,2,0:T(8,128)})) conditional(s32[]{:T(128)} %convert_element_type.106, (f32[4,1024]{1,0:T(4,128)S(1)}, f32[4,1024]{1,0:T(4,128)S(1)}, f32[4,1024,64]{1,2,0:T(8,128)}) %tuple.62, (s32[]{:T(128)}, s32[]{:T(128)}, s32[]{:T(128)}, ...), branch_computations={%region_4.4_spmd, %region_5.7_spmd} | conditional | flops 1923098624 | bytes 107565224 | solution.py:115
  334.2 2.1 convolution_convert_fusion
  337.3 2.4 fusion.15
  339.7 9.2 %fusion.40 = (f32[4,1024]{1,0:T(4,128)S(1)}, f32[4,1024,1024]{1,2,0:T(8,128)}) fusion(bf16[1024,4,32]{0,2,1:T(8,128)(2,1)S(1)} %get-tuple-element.258, bf16[8,1024,32]{1,2,0:T(8,128)(2,1)} %get-tuple-element.257, s32[]{:T(128)S(6)} %select_n.18, f32[4,1024,1024]{2,1,0:T(8,128)S(1)} %fusion.15, pred[1024,1024]{0,1:T(8,128)(4,1)} %broadcast_compare_fusion), kind=kOutput, calls=%fused_computation.67 | convolution fusion | flops 285208576 | bytes 34947076 | tf_op jit(solution)/shard_map/while/body/eval_jaxpr/cond/branch_1_fun/qhd,kd->hqk/dot_general | solution.py:96
  348.9 9.2 %fusion.5 = f32[4,1024]{1,0:T(4,128)S(1)} fusion(f32[4,1024,1024]{1,2,0:T(8,128)} %get-tuple-element.389, f32[4,1024]{1,0:T(4,128)S(1)} %max.5, pred[1024,1024]{0,1:T(8,128)(4,1)} %broadcast_compare_fusion), kind=kLoop, calls=%fused_computation.6 | loop fusion | flops 12578816 | bytes 17858560 | tf_op jit(solution)/shard_map/while/body/eval_jaxpr/cond/branch_1_fun/reduce_sum | solution.py:106
  358.1 8.8 %fusion.9 = f32[4,1024,64]{1,2,0:T(8,128)} fusion(f32[4,1024,1024]{1,2,0:T(8,128)} %get-tuple-element.389, f32[4,1024]{1,0:T(4,128)S(1)} %max.5, pred[1024,1024]{0,1:T(8,128)(4,1)S(1)} %copy-done.2, f32[4,1024,64]{1,2,0:T(8,128)} %get-tuple-element.260, bf16[1024,4,128]{0,2,1:T(8,128)(2,1)S(1)} %bitcast.42, f32[4,1024]{1,0:T(4,128)S(1)} %get-tuple-element.387), kind=kOutput, calls=%fused_computation.11 | convolution fusion | flops 549978112 | bytes 20480000 | tf_op jit(solution)/shard_map/while/body/eval_jaxpr/cond/branch_1_fun/hqk,khd->hqd/dot_general | solution.py:107
  368.2 36.4 %conditional.3 = ((f32[4,1024]{1,0:T(4,128)S(1)}, f32[4,1024]{1,0:T(4,128)S(1)}, f32[4,1024,64]{1,2,0:T(8,128)})) conditional(s32[]{:T(128)} %convert_element_type.106, (f32[4,1024]{1,0:T(4,128)S(1)}, f32[4,1024]{1,0:T(4,128)S(1)}, f32[4,1024,64]{1,2,0:T(8,128)}) %tuple.62, (s32[]{:T(128)}, s32[]{:T(128)}, s32[]{:T(128)}, ...), branch_computations={%region_4.4_spmd, %region_5.7_spmd} | conditional | flops 1923098624 | bytes 107565224 | solution.py:115
  370.3 1.7 broadcast_compare_fusion
  372.0 2.1 convolution_convert_fusion
  375.1 2.4 fusion.15
  377.5 9.2 %fusion.40 = (f32[4,1024]{1,0:T(4,128)S(1)}, f32[4,1024,1024]{1,2,0:T(8,128)}) fusion(bf16[1024,4,32]{0,2,1:T(8,128)(2,1)S(1)} %get-tuple-element.258, bf16[8,1024,32]{1,2,0:T(8,128)(2,1)} %get-tuple-element.257, s32[]{:T(128)S(6)} %select_n.18, f32[4,1024,1024]{2,1,0:T(8,128)S(1)} %fusion.15, pred[1024,1024]{0,1:T(8,128)(4,1)} %broadcast_compare_fusion), kind=kOutput, calls=%fused_computation.67 | convolution fusion | flops 285208576 | bytes 34947076 | tf_op jit(solution)/shard_map/while/body/eval_jaxpr/cond/branch_1_fun/qhd,kd->hqk/dot_general | solution.py:96
  386.7 9.2 %fusion.5 = f32[4,1024]{1,0:T(4,128)S(1)} fusion(f32[4,1024,1024]{1,2,0:T(8,128)} %get-tuple-element.389, f32[4,1024]{1,0:T(4,128)S(1)} %max.5, pred[1024,1024]{0,1:T(8,128)(4,1)} %broadcast_compare_fusion), kind=kLoop, calls=%fused_computation.6 | loop fusion | flops 12578816 | bytes 17858560 | tf_op jit(solution)/shard_map/while/body/eval_jaxpr/cond/branch_1_fun/reduce_sum | solution.py:106
  395.9 8.8 %fusion.9 = f32[4,1024,64]{1,2,0:T(8,128)} fusion(f32[4,1024,1024]{1,2,0:T(8,128)} %get-tuple-element.389, f32[4,1024]{1,0:T(4,128)S(1)} %max.5, pred[1024,1024]{0,1:T(8,128)(4,1)S(1)} %copy-done.2, f32[4,1024,64]{1,2,0:T(8,128)} %get-tuple-element.260, bf16[1024,4,128]{0,2,1:T(8,128)(2,1)S(1)} %bitcast.42, f32[4,1024]{1,0:T(4,128)S(1)} %get-tuple-element.387), kind=kOutput, calls=%fused_computation.11 | convolution fusion | flops 549978112 | bytes 20480000 | tf_op jit(solution)/shard_map/while/body/eval_jaxpr/cond/branch_1_fun/hqk,khd->hqd/dot_general | solution.py:107
  406.0 36.4 %conditional.3 = ((f32[4,1024]{1,0:T(4,128)S(1)}, f32[4,1024]{1,0:T(4,128)S(1)}, f32[4,1024,64]{1,2,0:T(8,128)})) conditional(s32[]{:T(128)} %convert_element_type.106, (f32[4,1024]{1,0:T(4,128)S(1)}, f32[4,1024]{1,0:T(4,128)S(1)}, f32[4,1024,64]{1,2,0:T(8,128)}) %tuple.62, (s32[]{:T(128)}, s32[]{:T(128)}, s32[]{:T(128)}, ...), branch_computations={%region_4.4_spmd, %region_5.7_spmd} | conditional | flops 1923098624 | bytes 107565224 | solution.py:115
  409.8 2.1 convolution_convert_fusion
  412.9 2.4 fusion.15
  415.3 9.2 %fusion.40 = (f32[4,1024]{1,0:T(4,128)S(1)}, f32[4,1024,1024]{1,2,0:T(8,128)}) fusion(bf16[1024,4,32]{0,2,1:T(8,128)(2,1)S(1)} %get-tuple-element.258, bf16[8,1024,32]{1,2,0:T(8,128)(2,1)} %get-tuple-element.257, s32[]{:T(128)S(6)} %select_n.18, f32[4,1024,1024]{2,1,0:T(8,128)S(1)} %fusion.15, pred[1024,1024]{0,1:T(8,128)(4,1)} %broadcast_compare_fusion), kind=kOutput, calls=%fused_computation.67 | convolution fusion | flops 285208576 | bytes 34947076 | tf_op jit(solution)/shard_map/while/body/eval_jaxpr/cond/branch_1_fun/qhd,kd->hqk/dot_general | solution.py:96
  424.5 9.2 %fusion.5 = f32[4,1024]{1,0:T(4,128)S(1)} fusion(f32[4,1024,1024]{1,2,0:T(8,128)} %get-tuple-element.389, f32[4,1024]{1,0:T(4,128)S(1)} %max.5, pred[1024,1024]{0,1:T(8,128)(4,1)} %broadcast_compare_fusion), kind=kLoop, calls=%fused_computation.6 | loop fusion | flops 12578816 | bytes 17858560 | tf_op jit(solution)/shard_map/while/body/eval_jaxpr/cond/branch_1_fun/reduce_sum | solution.py:106
  433.7 8.8 %fusion.9 = f32[4,1024,64]{1,2,0:T(8,128)} fusion(f32[4,1024,1024]{1,2,0:T(8,128)} %get-tuple-element.389, f32[4,1024]{1,0:T(4,128)S(1)} %max.5, pred[1024,1024]{0,1:T(8,128)(4,1)S(1)} %copy-done.2, f32[4,1024,64]{1,2,0:T(8,128)} %get-tuple-element.260, bf16[1024,4,128]{0,2,1:T(8,128)(2,1)S(1)} %bitcast.42, f32[4,1024]{1,0:T(4,128)S(1)} %get-tuple-element.387), kind=kOutput, calls=%fused_computation.11 | convolution fusion | flops 549978112 | bytes 20480000 | tf_op jit(solution)/shard_map/while/body/eval_jaxpr/cond/branch_1_fun/hqk,khd->hqd/dot_general | solution.py:107
  443.8 36.4 %conditional.3 = ((f32[4,1024]{1,0:T(4,128)S(1)}, f32[4,1024]{1,0:T(4,128)S(1)}, f32[4,1024,64]{1,2,0:T(8,128)})) conditional(s32[]{:T(128)} %convert_element_type.106, (f32[4,1024]{1,0:T(4,128)S(1)}, f32[4,1024]{1,0:T(4,128)S(1)}, f32[4,1024,64]{1,2,0:T(8,128)}) %tuple.62, (s32[]{:T(128)}, s32[]{:T(128)}, s32[]{:T(128)}, ...), branch_computations={%region_4.4_spmd, %region_5.7_spmd} | conditional | flops 1923098624 | bytes 107565224 | solution.py:115
  447.6 2.1 convolution_convert_fusion
  450.7 2.4 fusion.15
  453.1 9.2 %fusion.40 = (f32[4,1024]{1,0:T(4,128)S(1)}, f32[4,1024,1024]{1,2,0:T(8,128)}) fusion(bf16[1024,4,32]{0,2,1:T(8,128)(2,1)S(1)} %get-tuple-element.258, bf16[8,1024,32]{1,2,0:T(8,128)(2,1)} %get-tuple-element.257, s32[]{:T(128)S(6)} %select_n.18, f32[4,1024,1024]{2,1,0:T(8,128)S(1)} %fusion.15, pred[1024,1024]{0,1:T(8,128)(4,1)} %broadcast_compare_fusion), kind=kOutput, calls=%fused_computation.67 | convolution fusion | flops 285208576 | bytes 34947076 | tf_op jit(solution)/shard_map/while/body/eval_jaxpr/cond/branch_1_fun/qhd,kd->hqk/dot_general | solution.py:96
  462.3 9.2 %fusion.5 = f32[4,1024]{1,0:T(4,128)S(1)} fusion(f32[4,1024,1024]{1,2,0:T(8,128)} %get-tuple-element.389, f32[4,1024]{1,0:T(4,128)S(1)} %max.5, pred[1024,1024]{0,1:T(8,128)(4,1)} %broadcast_compare_fusion), kind=kLoop, calls=%fused_computation.6 | loop fusion | flops 12578816 | bytes 17858560 | tf_op jit(solution)/shard_map/while/body/eval_jaxpr/cond/branch_1_fun/reduce_sum | solution.py:106
  471.5 8.8 %fusion.9 = f32[4,1024,64]{1,2,0:T(8,128)} fusion(f32[4,1024,1024]{1,2,0:T(8,128)} %get-tuple-element.389, f32[4,1024]{1,0:T(4,128)S(1)} %max.5, pred[1024,1024]{0,1:T(8,128)(4,1)S(1)} %copy-done.2, f32[4,1024,64]{1,2,0:T(8,128)} %get-tuple-element.260, bf16[1024,4,128]{0,2,1:T(8,128)(2,1)S(1)} %bitcast.42, f32[4,1024]{1,0:T(4,128)S(1)} %get-tuple-element.387), kind=kOutput, calls=%fused_computation.11 | convolution fusion | flops 549978112 | bytes 20480000 | tf_op jit(solution)/shard_map/while/body/eval_jaxpr/cond/branch_1_fun/hqk,khd->hqd/dot_general | solution.py:107
  481.6 36.4 %conditional.3 = ((f32[4,1024]{1,0:T(4,128)S(1)}, f32[4,1024]{1,0:T(4,128)S(1)}, f32[4,1024,64]{1,2,0:T(8,128)})) conditional(s32[]{:T(128)} %convert_element_type.106, (f32[4,1024]{1,0:T(4,128)S(1)}, f32[4,1024]{1,0:T(4,128)S(1)}, f32[4,1024,64]{1,2,0:T(8,128)}) %tuple.62, (s32[]{:T(128)}, s32[]{:T(128)}, s32[]{:T(128)}, ...), branch_computations={%region_4.4_spmd, %region_5.7_spmd} | conditional | flops 1923098624 | bytes 107565224 | solution.py:115
  485.4 2.1 convolution_convert_fusion
  488.5 2.4 fusion.15
  490.9 9.2 %fusion.40 = (f32[4,1024]{1,0:T(4,128)S(1)}, f32[4,1024,1024]{1,2,0:T(8,128)}) fusion(bf16[1024,4,32]{0,2,1:T(8,128)(2,1)S(1)} %get-tuple-element.258, bf16[8,1024,32]{1,2,0:T(8,128)(2,1)} %get-tuple-element.257, s32[]{:T(128)S(6)} %select_n.18, f32[4,1024,1024]{2,1,0:T(8,128)S(1)} %fusion.15, pred[1024,1024]{0,1:T(8,128)(4,1)} %broadcast_compare_fusion), kind=kOutput, calls=%fused_computation.67 | convolution fusion | flops 285208576 | bytes 34947076 | tf_op jit(solution)/shard_map/while/body/eval_jaxpr/cond/branch_1_fun/qhd,kd->hqk/dot_general | solution.py:96
  500.1 9.2 %fusion.5 = f32[4,1024]{1,0:T(4,128)S(1)} fusion(f32[4,1024,1024]{1,2,0:T(8,128)} %get-tuple-element.389, f32[4,1024]{1,0:T(4,128)S(1)} %max.5, pred[1024,1024]{0,1:T(8,128)(4,1)} %broadcast_compare_fusion), kind=kLoop, calls=%fused_computation.6 | loop fusion | flops 12578816 | bytes 17858560 | tf_op jit(solution)/shard_map/while/body/eval_jaxpr/cond/branch_1_fun/reduce_sum | solution.py:106
  509.3 8.8 %fusion.9 = f32[4,1024,64]{1,2,0:T(8,128)} fusion(f32[4,1024,1024]{1,2,0:T(8,128)} %get-tuple-element.389, f32[4,1024]{1,0:T(4,128)S(1)} %max.5, pred[1024,1024]{0,1:T(8,128)(4,1)S(1)} %copy-done.2, f32[4,1024,64]{1,2,0:T(8,128)} %get-tuple-element.260, bf16[1024,4,128]{0,2,1:T(8,128)(2,1)S(1)} %bitcast.42, f32[4,1024]{1,0:T(4,128)S(1)} %get-tuple-element.387), kind=kOutput, calls=%fused_computation.11 | convolution fusion | flops 549978112 | bytes 20480000 | tf_op jit(solution)/shard_map/while/body/eval_jaxpr/cond/branch_1_fun/hqk,khd->hqd/dot_general | solution.py:107
  519.8 11.4 %all_to_all.16 = bf16[4,256,256]{1,2,0:T(8,128)(2,1)S(1)} all-to-all(bf16[4,256,256]{1,2,0:T(8,128)(2,1)S(1)} %copy.28), channel_id=1, replica_groups=mesh['sp'=8,'tp'=4] {'tp'}, dimensions={0} | all-to-all | bytes 1048576 | tf_op jit(solution)/shard_map/all_to_all | solution.py:142
  531.2 5.9 %multiply_reduce_fusion = (f32[256]{0:T(256)S(1)}, f32[256,4096]{1,0:T(8,128)S(1)}) fusion(bf16[256,1024]{0,1:T(8,128)(2,1)S(1)} %bitcast.47, bf16[1024,4096]{1,0:T(8,128)(2,1)} %param.24), kind=kOutput, calls=%fused_computation.32 | convolution fusion | flops 2149580544 | bytes 13108224 | tf_op jit(solution)/shard_map/dot_general | solution.py:143
  537.2 1.9 multiply_convert_fusion
  (151 shorter events, 33.1 us)
Async XLA Ops:
  6.5 47.9 %copy-start = (bf16[768,384]{1,0:T(8,128)(2,1)S(1)}, bf16[768,384]{1,0:T(8,128)(2,1)}, u32[]{:S(2)}) copy-start(bf16[768,384]{1,0:T(8,128)(2,1)} %param.22) | copy-start | bytes 1769476
  6.5 26.4 %all-gather.4.cloned.1.call-start = ((), (), s32[]{:S(2)}) async-start(), calls=%async_computation.1 | async-start | bytes 1310720 | tf_op jit(solution)/shard_map/all_gather | solution.py:65
  8.7 4.4 copy-start.8
  8.7 5.3 copy-start.5
  8.7 5.3 copy-start.10
  13.9 4.8 copy-start.7
  14.0 5.8 %copy-start.9 = (bf16[4096,32]{0,1:T(8,128)(2,1)S(1)}, bf16[4096,32]{0,1:T(8,128)(2,1)}, u32[]{:S(2)}) copy-start(bf16[4096,32]{0,1:T(8,128)(2,1)} %param.19) | copy-start | bytes 786436
  14.0 40.4 %all-gather.8.cloned.1.call-start = ((), (), s32[]{:S(2)}) async-start(), calls=%async_computation.3 | async-start | bytes 1966080 | tf_op jit(solution)/shard_map/all_gather | solution.py:64
  19.7 184.6 %all-gather.6.cloned.1.call-start = ((), (), s32[]{:S(2)}) async-start(), calls=%async_computation.2 | async-start | bytes 11796480 | tf_op jit(solution)/shard_map/all_gather | solution.py:125
  204.3 1.6 slice-start
  223.0 1.0 copy-start.3
  235.5 9.2 %copy-start.2 = (pred[1024,1024]{0,1:T(8,128)(4,1)S(1)}, pred[1024,1024]{0,1:T(8,128)(4,1)}, u32[]{:S(2)}) copy-start(pred[1024,1024]{0,1:T(8,128)(4,1)} %broadcast_compare_fusion) | copy-start | bytes 3145732 | tf_op jit(solution)/shard_map/while/body/eval_jaxpr/cond
  235.5 9.2 %copy-start.4 = (bf16[1024,512]{0,1:T(8,128)(2,1)S(1)}, bf16[1024,512]{0,1:T(8,128)(2,1)}, u32[]{:S(2)}) copy-start(bf16[1024,512]{0,1:T(8,128)(2,1)} %copy-done.3) | copy-start | bytes 3145732 | tf_op jit(solution)/shard_map/while/body/eval_jaxpr/cond
  260.8 1.0 copy-start.3
  273.3 9.2 %copy-start.2 = (pred[1024,1024]{0,1:T(8,128)(4,1)S(1)}, pred[1024,1024]{0,1:T(8,128)(4,1)}, u32[]{:S(2)}) copy-start(pred[1024,1024]{0,1:T(8,128)(4,1)} %broadcast_compare_fusion) | copy-start | bytes 3145732 | tf_op jit(solution)/shard_map/while/body/eval_jaxpr/cond
  273.3 9.2 %copy-start.4 = (bf16[1024,512]{0,1:T(8,128)(2,1)S(1)}, bf16[1024,512]{0,1:T(8,128)(2,1)}, u32[]{:S(2)}) copy-start(bf16[1024,512]{0,1:T(8,128)(2,1)} %copy-done.3) | copy-start | bytes 3145732 | tf_op jit(solution)/shard_map/while/body/eval_jaxpr/cond
  298.5 1.0 copy-start.3
  311.1 9.2 %copy-start.2 = (pred[1024,1024]{0,1:T(8,128)(4,1)S(1)}, pred[1024,1024]{0,1:T(8,128)(4,1)}, u32[]{:S(2)}) copy-start(pred[1024,1024]{0,1:T(8,128)(4,1)} %broadcast_compare_fusion) | copy-start | bytes 3145732 | tf_op jit(solution)/shard_map/while/body/eval_jaxpr/cond
  311.1 9.2 %copy-start.4 = (bf16[1024,512]{0,1:T(8,128)(2,1)S(1)}, bf16[1024,512]{0,1:T(8,128)(2,1)}, u32[]{:S(2)}) copy-start(bf16[1024,512]{0,1:T(8,128)(2,1)} %copy-done.3) | copy-start | bytes 3145732 | tf_op jit(solution)/shard_map/while/body/eval_jaxpr/cond
  336.3 1.0 copy-start.3
  348.9 9.2 %copy-start.2 = (pred[1024,1024]{0,1:T(8,128)(4,1)S(1)}, pred[1024,1024]{0,1:T(8,128)(4,1)}, u32[]{:S(2)}) copy-start(pred[1024,1024]{0,1:T(8,128)(4,1)} %broadcast_compare_fusion) | copy-start | bytes 3145732 | tf_op jit(solution)/shard_map/while/body/eval_jaxpr/cond
  348.9 9.2 %copy-start.4 = (bf16[1024,512]{0,1:T(8,128)(2,1)S(1)}, bf16[1024,512]{0,1:T(8,128)(2,1)}, u32[]{:S(2)}) copy-start(bf16[1024,512]{0,1:T(8,128)(2,1)} %copy-done.3) | copy-start | bytes 3145732 | tf_op jit(solution)/shard_map/while/body/eval_jaxpr/cond
  374.1 1.0 copy-start.3
  386.7 9.2 %copy-start.2 = (pred[1024,1024]{0,1:T(8,128)(4,1)S(1)}, pred[1024,1024]{0,1:T(8,128)(4,1)}, u32[]{:S(2)}) copy-start(pred[1024,1024]{0,1:T(8,128)(4,1)} %broadcast_compare_fusion) | copy-start | bytes 3145732 | tf_op jit(solution)/shard_map/while/body/eval_jaxpr/cond
  386.7 9.2 %copy-start.4 = (bf16[1024,512]{0,1:T(8,128)(2,1)S(1)}, bf16[1024,512]{0,1:T(8,128)(2,1)}, u32[]{:S(2)}) copy-start(bf16[1024,512]{0,1:T(8,128)(2,1)} %copy-done.3) | copy-start | bytes 3145732 | tf_op jit(solution)/shard_map/while/body/eval_jaxpr/cond
  411.9 1.0 copy-start.3
  424.4 9.2 %copy-start.2 = (pred[1024,1024]{0,1:T(8,128)(4,1)S(1)}, pred[1024,1024]{0,1:T(8,128)(4,1)}, u32[]{:S(2)}) copy-start(pred[1024,1024]{0,1:T(8,128)(4,1)} %broadcast_compare_fusion) | copy-start | bytes 3145732 | tf_op jit(solution)/shard_map/while/body/eval_jaxpr/cond
  424.5 9.2 %copy-start.4 = (bf16[1024,512]{0,1:T(8,128)(2,1)S(1)}, bf16[1024,512]{0,1:T(8,128)(2,1)}, u32[]{:S(2)}) copy-start(bf16[1024,512]{0,1:T(8,128)(2,1)} %copy-done.3) | copy-start | bytes 3145732 | tf_op jit(solution)/shard_map/while/body/eval_jaxpr/cond
  449.7 1.0 copy-start.3
  462.2 9.2 %copy-start.2 = (pred[1024,1024]{0,1:T(8,128)(4,1)S(1)}, pred[1024,1024]{0,1:T(8,128)(4,1)}, u32[]{:S(2)}) copy-start(pred[1024,1024]{0,1:T(8,128)(4,1)} %broadcast_compare_fusion) | copy-start | bytes 3145732 | tf_op jit(solution)/shard_map/while/body/eval_jaxpr/cond
  462.2 9.2 %copy-start.4 = (bf16[1024,512]{0,1:T(8,128)(2,1)S(1)}, bf16[1024,512]{0,1:T(8,128)(2,1)}, u32[]{:S(2)}) copy-start(bf16[1024,512]{0,1:T(8,128)(2,1)} %copy-done.3) | copy-start | bytes 3145732 | tf_op jit(solution)/shard_map/while/body/eval_jaxpr/cond
  487.5 1.0 copy-start.3
  500.0 9.2 %copy-start.2 = (pred[1024,1024]{0,1:T(8,128)(4,1)S(1)}, pred[1024,1024]{0,1:T(8,128)(4,1)}, u32[]{:S(2)}) copy-start(pred[1024,1024]{0,1:T(8,128)(4,1)} %broadcast_compare_fusion) | copy-start | bytes 3145732 | tf_op jit(solution)/shard_map/while/body/eval_jaxpr/cond
  500.0 9.2 %copy-start.4 = (bf16[1024,512]{0,1:T(8,128)(2,1)S(1)}, bf16[1024,512]{0,1:T(8,128)(2,1)}, u32[]{:S(2)}) copy-start(bf16[1024,512]{0,1:T(8,128)(2,1)} %copy-done.3) | copy-start | bytes 3145732 | tf_op jit(solution)/shard_map/while/body/eval_jaxpr/cond
  531.2 6.0 %copy-start.6 = (f32[4096]{0:T(1024)S(1)}, f32[4096]{0:T(1024)}, u32[]{:S(2)}) copy-start(f32[4096]{0:T(1024)} %param.25) | copy-start | bytes 49156
  531.2 7.9 %copy-start.1 = (bf16[768,384]{1,0:T(8,128)(2,1)S(1)}, bf16[768,384]{1,0:T(8,128)(2,1)}, u32[]{:S(2)}) copy-start(bf16[768,384]{1,0:T(8,128)(2,1)} %param.22) | copy-start | bytes 1769476
Sparse Core Ops, SparseCore 0:
  14.1 18.8 all-gather.3
  34.5 19.9 all-gather.7
  56.6 147.6 all-gather.5
